TPU v7x, 32 devices: a whole 2x2x4 slice. The times are simulated.
32 devices in a mesh: grp: 2 (over y), sp: 4 (over z), tp: 4 (over x, core).
Axes of the slice: x: 2, y: 2, z: 4, core: 2. Of those that a mesh axis runs over, the one named last changes fastest.
Arguments:
- tokens: bfloat16 [6144, 2048], P(('grp', 'sp'), 'tp'), parts along dimension 0, may hold values from -8 to 8
- norm_gain: float32 [2, 2048], replicated, may hold values from 0.1 to 1.9
- w_value: bfloat16 [2, 2048, 2048], P(None, 'sp', 'tp'), may hold values from -0.125 to 0.125
- w_gate: bfloat16 [2, 2048, 2048], P(None, 'sp', 'tp'), may hold values from -0.125 to 0.125
- taps: float32 [2, 31, 2048], P(None, None, 'tp'), may hold values from -2 to 2
- ln_gain: float32 [2, 2048], P(None, 'tp'), may hold values from 0.1 to 1.9
- ln_shift: float32 [2, 2048], P(None, 'tp'), may hold values from -3 to 3
- w_out: bfloat16 [2, 2048, 2048], P(None, 'sp', 'tp'), may hold values from -0.125 to 0.125
Outputs:
- stream_out: bfloat16 [6144, 2048], P(('grp', 'sp'), 'tp'), parts along dimension 0
There are 2 independent parts, one for each index of `grp`. A program takes and returns all parts, laid end to end along the dimension named above; an argument that names none is the same for every part. Nothing has to cross between parts.
All inputs are finite; a program needn't handle non-finite values.
Results may differ from a plain program's by a relative error of at most 0.012.
Values may be sent and summed in bfloat16 or wider, within the bound.
A program may use at most 64 MiB of HBM per device.

v0:
```python
import jax
import jax.numpy as jnp
from jax import lax
from jax.sharding import PartitionSpec as P


def padded_2(block, sides, width):
    for axis, dim in sides:
        count = lax.axis_size(axis)
        forward = [(i, i + 1) for i in range(count - 1)]
        backward = [(target, source) for source, target in forward]
        low = lax.ppermute(
            lax.slice_in_dim(block, block.shape[dim] - width, None, axis=dim), axis, forward
        )
        high = lax.ppermute(lax.slice_in_dim(block, 0, width, axis=dim), axis, backward)
        block = jnp.concatenate([low, block, high], axis=dim)
    return block


def shards(tokens, norm_gain, w_value, w_gate, taps, ln_gain, ln_shift, w_out):
    layers = w_value.shape[0]
    kernel = taps.shape[1]
    half = (kernel - 1) // 2
    count = tokens.shape[0]
    every = (
        lax.all_gather(w_value, "sp", axis=1, tiled=True),
        lax.all_gather(w_gate, "sp", axis=1, tiled=True),
        lax.all_gather(w_out, "sp", axis=1, tiled=True),
    )
    stream = tokens
    for layer in range(layers):
        val_rows, gate_rows, out_rows = (every[0][layer], every[1][layer], every[2][layer])
        chan_dev = val_rows.shape[1]
        whole = lax.all_gather(stream, "tp", axis=1, tiled=True).astype(jnp.float32)
        meansq = jnp.mean(whole * whole, axis=1, keepdims=True)
        normed = (whole * lax.rsqrt(meansq + 1e-06) * norm_gain[layer]).astype(jnp.bfloat16)
        value = jnp.dot(normed, val_rows, preferred_element_type=jnp.float32)
        gate = jnp.dot(normed, gate_rows, preferred_element_type=jnp.float32)
        glu = (value * jax.nn.sigmoid(gate)).astype(jnp.bfloat16)
        padded = padded_2(glu, (("sp", 0),), half).astype(jnp.float32)
        layer_taps = taps[layer]
        conv = jnp.zeros((count, chan_dev), jnp.float32)
        for step in range(kernel):
            conv = conv + layer_taps[step][None, :] * padded[step : step + count]
        totals, squared = lax.psum((jnp.sum(conv, axis=1), jnp.sum(conv * conv, axis=1)), "tp")
        chan_all = chan_dev * lax.axis_size("tp")
        mean_c = (totals / chan_all)[:, None]
        var_c = (squared / chan_all)[:, None] - mean_c * mean_c
        shaped = (conv - mean_c) * lax.rsqrt(var_c + 1e-05) * ln_gain[layer][None, :] + ln_shift[
            layer
        ][None, :]
        act = jax.nn.silu(shaped).astype(jnp.bfloat16)
        update = jnp.dot(
            lax.all_gather(act, "tp", axis=1, tiled=True),
            out_rows,
            preferred_element_type=jnp.float32,
        )
        stream = (stream.astype(jnp.float32) + update).astype(jnp.bfloat16)
    return stream


def solution(mesh):
    return jax.shard_map(
        shards,
        mesh=mesh,
        in_specs=(
            P(("grp", "sp"), "tp"),
            P(),
            P(None, "sp", "tp"),
            P(None, "sp", "tp"),
            P(None, None, "tp"),
            P(None, "tp"),
            P(None, "tp"),
            P(None, "sp", "tp"),
        ),
        out_specs=P(("grp", "sp"), "tp"),
        check_vma=False,
    )
```

profile of v0, /device:TPU:1, one launch (start us, length us, event | category | flops | bytes accessed | tf_op | source)
XLA Modules:
  0.0 418.1 jit_solution(12790074441776958482)
XLA Ops:
  9.6 30.3 %all-gather.8.cloned.1.call-done = bf16[768,2048]{1,0:T(8,128)(2,1)} async-done(((bf16[768,512]{1,0:T(8,128)(2,1)}), bf16[768,2048]{1,0:T(8,128)(2,1)}) %all-gather.8.cloned.1.call-update) | async-done | bytes 3145744 | tf_op jit(solution)/shard_map/all_gather | solution.py:34
  39.9 2.7 fusion
  42.6 79.1 %all-gather.12.cloned.1.call-done = bf16[2,2048,512]{2,1,0:T(8,128)(2,1)} async-done(((bf16[2,512,512]{2,1,0:T(8,128)(2,1)}), bf16[2,2048,512]{2,1,0:T(8,128)(2,1)}) %all-gather.12.cloned.1.call-update) | async-done | bytes 4194320 | tf_op jit(solution)/shard_map/all_gather | solution.py:27
  121.7 4.6 %fusion.10 = f32[768,512]{1,0:T(8,128)} fusion(bf16[2,2048,512]{2,1,0:T(8,128)(2,1)} %all-gather.12.cloned.1.call-done, bf16[768,2048]{1,0:T(8,128)(2,1)S(1)} %copy-done, f32[2048]{0:T(1024)S(1)} %bitcast.164, f32[768]{0:T(1024)S(1)} %add_rsqrt_fusion.3), kind=kOutput, calls=%fused_computation.19 | convolution fusion | flops 1616904192 | bytes 6827008 | tf_op jit(solution)/shard_map/dot_general | solution.py:38
  126.3 76.2 %all-gather.10.cloned.1.call-done = bf16[2,2048,512]{2,1,0:T(8,128)(2,1)} async-done(((bf16[2,512,512]{2,1,0:T(8,128)(2,1)}), bf16[2,2048,512]{2,1,0:T(8,128)(2,1)}) %all-gather.10.cloned.1.call-update) | async-done | bytes 4194320 | tf_op jit(solution)/shard_map/all_gather | solution.py:26
  202.5 4.0 multiply_convert_fusion.3
  209.2 3.2 collective-permute-done.1
  212.7 6.8 %fusion.77 = (f32[768]{0:T(1024)S(1)}, f32[768]{0:T(1024)S(1)}, f32[768,512]{1,0:T(8,128)S(1)}) fusion(f32[798,512]{1,0:T(8,128)S(1)} %maximum_convert_fusion, f32[512]{0:T(512)S(1)} %bitcast.130, f32[512]{0:T(512)S(1)} %bitcast.131, f32[512]{0:T(512)S(1)} %bitcast.132, f32[512]{0:T(512)S(1)} %bitcast.133, f32[512]{0:T(512)S(1)} %bitcast.134, ...), kind=kLoop, calls=%fused_computation.161 | loop fusion | flops 25164288 | bytes 50401280 | tf_op jit(solution)/shard_map/reduce_sum | solution.py:45
  219.5 7.3 %all-reduce.1 = (f32[768]{0:T(1024)S(1)}, f32[768]{0:T(1024)S(1)}) all-reduce(f32[768]{0:T(1024)S(1)} %get-tuple-element.8, f32[768]{0:T(1024)S(1)} %get-tuple-element.7), channel_id=1, replica_groups=mesh['grp'=2,'sp'=4,'tp'=4] {'tp'}, use_global_device_ids=true, to_apply=%region_4.0 | all-reduce | flops 1536 | bytes 12288 | tf_op jit(solution)/shard_map/psum | solution.py:45
  226.8 1.5 multiply_convert_fusion.2
  228.4 55.0 %all-gather.16.cloned.1.call-done = bf16[2,2048,512]{2,1,0:T(8,128)(2,1)} async-done(((bf16[2,512,512]{2,1,0:T(8,128)(2,1)}), bf16[2,2048,512]{2,1,0:T(8,128)(2,1)}) %all-gather.16.cloned.1.call-update) | async-done | bytes 4194320 | tf_op jit(solution)/shard_map/all_gather | solution.py:28
  283.4 28.8 %all-gather.14.cloned.1.call-done = bf16[768,2048]{1,0:T(8,128)(2,1)} async-done(((bf16[768,512]{1,0:T(8,128)(2,1)}), bf16[768,2048]{1,0:T(8,128)(2,1)}) %all-gather.14.cloned.1.call-update) | async-done | bytes 3145744 | tf_op jit(solution)/shard_map/all_gather | solution.py:54
  312.2 5.2 %add_convert_fusion.1 = bf16[768,512]{1,0:T(8,128)(2,1)} fusion(bf16[768,512]{1,0:T(8,128)(2,1)S(1)} %copy-done.2, bf16[768,2048]{1,0:T(8,128)(2,1)} %all-gather.14.cloned.1.call-done, bf16[2,2048,512]{2,1,0:T(8,128)(2,1)} %all-gather.16.cloned.1.call-done), kind=kOutput, calls=%fused_computation.148 | convolution fusion | flops 1611792384 | bytes 6815744 | tf_op jit(solution)/shard_map/dot_general | solution.py:53
  317.7 28.4 %all-gather.18.cloned.1.call-done = bf16[768,2048]{1,0:T(8,128)(2,1)} async-done(((bf16[768,512]{1,0:T(8,128)(2,1)}), bf16[768,2048]{1,0:T(8,128)(2,1)}) %all-gather.18.cloned.1.call-update) | async-done | bytes 3145744 | tf_op jit(solution)/shard_map/all_gather | solution.py:34
  346.1 2.7 fusion.3
  348.9 3.6 fusion.7
  352.5 2.0 multiply_convert_fusion.1
  354.6 3.1 collective-permute-start.2
  359.1 3.1 collective-permute-done.3
  362.4 6.8 %fusion.76 = (f32[768]{0:T(1024)S(1)}, f32[768]{0:T(1024)S(1)}, f32[768,512]{1,0:T(8,128)S(1)}) fusion(f32[798,512]{1,0:T(8,128)S(1)} %maximum_convert_fusion.1, f32[512]{0:T(512)S(1)} %bitcast.96, f32[512]{0:T(512)S(1)} %bitcast.97, f32[512]{0:T(512)S(1)} %bitcast.140, f32[512]{0:T(512)S(1)} %bitcast.141, f32[512]{0:T(512)S(1)} %bitcast.142, ...), kind=kLoop, calls=%fused_computation.160 | loop fusion | flops 25164288 | bytes 50401280 | tf_op jit(solution)/shard_map/reduce_sum | solution.py:45
  369.2 6.8 %all-reduce = (f32[768]{0:T(1024)S(1)}, f32[768]{0:T(1024)S(1)}) all-reduce(f32[768]{0:T(1024)S(1)} %get-tuple-element.6, f32[768]{0:T(1024)S(1)} %get-tuple-element.5), channel_id=1, replica_groups=mesh['grp'=2,'sp'=4,'tp'=4] {'tp'}, use_global_device_ids=true, to_apply=%region_9.10 | all-reduce | flops 1536 | bytes 12288 | tf_op jit(solution)/shard_map/psum | solution.py:45
  376.0 1.5 multiply_convert_fusion
  377.6 28.5 %all-gather.20.cloned.1.call-done = bf16[768,2048]{1,0:T(8,128)(2,1)} async-done(((bf16[768,512]{1,0:T(8,128)(2,1)}), bf16[768,2048]{1,0:T(8,128)(2,1)}) %all-gather.20.cloned.1.call-update) | async-done | bytes 3145744 | tf_op jit(solution)/shard_map/all_gather | solution.py:54
  406.1 5.2 %add_convert_fusion = bf16[768,512]{1,0:T(8,128)(2,1)} fusion(bf16[768,512]{1,0:T(8,128)(2,1)S(1)} %copy-done.3, bf16[768,2048]{1,0:T(8,128)(2,1)} %all-gather.20.cloned.1.call-done, bf16[2,2048,512]{2,1,0:T(8,128)(2,1)} %all-gather.16.cloned.1.call-done), kind=kOutput, calls=%fused_computation.144 | convolution fusion | flops 1611792384 | bytes 6815744 | tf_op jit(solution)/shard_map/dot_general | solution.py:53
  (52 shorter events, 7.8 us)
Async XLA Ops:
  6.5 33.4 %all-gather.8.cloned.1.call-start = ((), (), s32[]{:S(2)}) async-start(), calls=%async_computation | async-start | bytes 3932160 | tf_op jit(solution)/shard_map/all_gather | solution.py:34
  7.3 2.1 copy-start.6
  7.3 2.2 copy-start.4
  7.3 2.3 copy-start.5
  7.3 114.4 %all-gather.12.cloned.1.call-start = ((), (), s32[]{:S(2)}) async-start(), calls=%async_computation.2 | async-start | bytes 5242880 | tf_op jit(solution)/shard_map/all_gather | solution.py:27
  8.0 194.5 %all-gather.10.cloned.1.call-start = ((), (), s32[]{:S(2)}) async-start(), calls=%async_computation.1 | async-start | bytes 5242880 | tf_op jit(solution)/shard_map/all_gather | solution.py:26
  8.8 274.6 %all-gather.16.cloned.1.call-start = ((), (), s32[]{:S(2)}) async-start(), calls=%async_computation.4 | async-start | bytes 5242880 | tf_op jit(solution)/shard_map/all_gather | solution.py:28
  9.3 302.9 %all-gather.14.cloned.1.call-start = ((), (), s32[]{:S(2)}) async-start(), calls=%async_computation.3 | async-start | bytes 3932160 | tf_op jit(solution)/shard_map/all_gather | solution.py:54
  39.9 81.8 %copy-start = (bf16[768,2048]{1,0:T(8,128)(2,1)S(1)}, bf16[768,2048]{1,0:T(8,128)(2,1)}, u32[]{:S(2)}) copy-start(bf16[768,2048]{1,0:T(8,128)(2,1)} %all-gather.8.cloned.1.call-done) | copy-start | bytes 9437188
  126.3 82.9 %copy-start.7 = (f32[2,512]{1,0:T(2,128)S(1)}, f32[2,512]{1,0:T(2,128)}, u32[]{:S(2)}) copy-start(f32[2,512]{1,0:T(2,128)} %param.14) | copy-start | bytes 12292
  206.6 2.6 collective-permute-start
  207.9 4.5 %collective-permute-start.1 = (bf16[15,512]{1,0:T(8,128)(2,1)S(1)}, bf16[15,512]{1,0:T(8,128)(2,1)S(1)}, u32[]{:S(2)}, u32[]{:S(2)}) collective-permute-start(bf16[15,512]{1,0:T(8,128)(2,1)S(1)} %get-tuple-element.18), channel_id=1, source_target_pairs={{4,0},{8,4},{12,8},{5,1},{9,5},{13,9},{6,2},{10,6},{14,10},{7,3},{... | collective-permute-start | bytes 46088 | tf_op jit(solution)/shard_map/ppermute | solution.py:15
  226.8 85.4 %copy-start.2 = (bf16[768,512]{1,0:T(8,128)(2,1)S(1)}, bf16[768,512]{1,0:T(8,128)(2,1)}, u32[]{:S(2)}) copy-start(bf16[768,512]{1,0:T(8,128)(2,1)} %param.8) | copy-start | bytes 2359300
  228.3 117.8 %all-gather.18.cloned.1.call-start = ((), (), s32[]{:S(2)}) async-start(), calls=%async_computation.5 | async-start | bytes 3932160 | tf_op jit(solution)/shard_map/all_gather | solution.py:34
  317.4 88.6 %all-gather.20.cloned.1.call-start = ((), (), s32[]{:S(2)}) async-start(), calls=%async_computation.6 | async-start | bytes 3932160 | tf_op jit(solution)/shard_map/all_gather | solution.py:54
  346.1 2.8 copy-start.1
  348.9 3.6 copy-start.8
  354.6 4.5 %collective-permute-start.2 = (bf16[15,512]{1,0:T(8,128)(2,1)S(1)}, bf16[15,512]{1,0:T(8,128)(2,1)S(1)}, u32[]{:S(2)}, u32[]{:S(2)}) collective-permute-start(bf16[15,512]{1,0:T(8,128)(2,1)S(1)} %get-tuple-element.15), channel_id=1, source_target_pairs={{0,4},{4,8},{8,12},{1,5},{5,9},{9,13},{2,6},{6,10},{10,14},{3,7},{... | collective-permute-start | bytes 46088 | tf_op jit(solution)/shard_map/ppermute | solution.py:12
  357.7 4.5 %collective-permute-start.3 = (bf16[15,512]{1,0:T(8,128)(2,1)S(1)}, bf16[15,512]{1,0:T(8,128)(2,1)S(1)}, u32[]{:S(2)}, u32[]{:S(2)}) collective-permute-start(bf16[15,512]{1,0:T(8,128)(2,1)S(1)} %get-tuple-element.16), channel_id=1, source_target_pairs={{4,0},{8,4},{12,8},{5,1},{9,5},{13,9},{6,2},{10,6},{14,10},{7,3},{... | collective-permute-start | bytes 46088 | tf_op jit(solution)/shard_map/ppermute | solution.py:15
  376.0 30.1 %copy-start.3 = (bf16[768,512]{1,0:T(8,128)(2,1)S(1)}, bf16[768,512]{1,0:T(8,128)(2,1)}, u32[]{:S(2)}) copy-start(bf16[768,512]{1,0:T(8,128)(2,1)} %add_convert_fusion.1) | copy-start | bytes 2359300
Sparse Core Ops, SparseCore 0:
  8.9 30.9 all-gather.7
  41.5 80.1 all-gather.11
  123.3 79.2 all-gather.9
  204.0 79.3 all-gather.15
  284.8 27.3 all-gather.13
  317.6 28.4 all-gather.17
  377.7 28.3 all-gather.19
where the time goes:
time: 419 us; the launch traced here: 418 us
  waiting for transfers between devices  335 us (80%)
  matrix products  24.7 us (6%)
  other arithmetic  22.5 us (5%)
  blocking collectives  14.1 us (3%)
  between operations  13.8 us (3%)
  starting transfers between devices  7.4 us (2%)
    all_gather x1, waiting for transfers between devices, shards(): lax.all_gather(w_gate, 'sp', axis=1, tiled=True)  79.1 us
    all_gather x1, waiting for transfers between devices, shards(): lax.all_gather(w_value, 'sp', axis=1, tiled=True)  76.2 us
    all_gather x2, waiting for transfers between devices, shards(): whole = lax.all_gather(stream, 'tp', axis=1, tiled=True).astype(jnp.float32)  58.8 us
    all_gather x2, waiting for transfers between devices, shards(): lax.all_gather(act, 'tp', axis=1, tiled=True)  57.3 us
    all_gather x1, waiting for transfers between devices, shards(): lax.all_gather(w_out, 'sp', axis=1, tiled=True)  55 us
    psum x2, blocking collectives, shards(): lax.psum((jnp.sum(conv, axis=1), jnp.sum(conv * conv, axis=1)), 'tp')  14.1 us
    reduce_sum x2, other arithmetic, shards(): jnp.sum(conv, axis=1)  13.5 us
    dot_general x2, matrix products, shards(): jnp.dot(lax.all_gather(act, 'tp', axis=1, tiled=True), out_rows, preferre...  10.4 us
  transfers between devices with their start and end apart: 11, of which 9 were waited for; matrix products, arithmetic and copies ran while one was open for 5% of the time, Pallas kernels for 0%

commit v1 on v0

v1 whole, which is shorter than its diff:
```python
import functools

import jax
import jax.numpy as jnp
from jax import lax
from jax.experimental import pallas as pl
from jax.experimental.pallas import tpu as pltpu
from jax.sharding import PartitionSpec as P

MESH = pl.DeviceIdType.MESH
HALO = 16
LANES = 128
BLOCK = 64


def body(
    sizes,
    tokens,
    norm_gain,
    w_value,
    w_gate,
    taps,
    ln_gain,
    ln_shift,
    w_out,
    out,
    weights,
    gathered,
    glu,
    conv,
    stats,
    load_sem,
    z_send,
    z_recv,
    y_send,
    y_recv,
    x_send,
    x_recv,
    s_send,
    s_recv,
    h_send,
    h_recv,
):
    groups, n, tp, chunks, subs = sizes
    chips = tp // 2
    grp, sp, me = lax.axis_index("grp"), lax.axis_index("sp"), lax.axis_index("tp")
    chip, core = me // 2, me % 2
    partner = chip * 2 + 1 - core
    layers, depth, cols = w_value.shape
    kernel = taps.shape[1]
    half = (kernel - 1) // 2
    count = tokens.shape[0]
    rows = count // chunks
    width = cols * tp
    pieces = layers * 3 * subs
    part = depth // (groups * subs)
    hops = n - 1
    per_matrix = subs * hops
    f32, bf16 = jnp.float32, jnp.bfloat16

    def aligned(value, unit):
        return pl.multiple_of(value, unit)

    barrier = pltpu.get_barrier_semaphore()
    for off in range(1, tp):
        pl.semaphore_signal(
            barrier, inc=1, device_id={"tp": (me + off) % tp}, device_id_type=MESH
        )
    for off in range(1, groups):
        pl.semaphore_signal(
            barrier, inc=1, device_id={"grp": (grp + off) % groups}, device_id_type=MESH
        )

    @pl.when(sp > 0)
    def _():
        pl.semaphore_signal(barrier, inc=1, device_id={"sp": sp - 1}, device_id_type=MESH)

    @pl.when(sp < n - 1)
    def _():
        pl.semaphore_signal(barrier, inc=1, device_id={"sp": sp + 1}, device_id_type=MESH)

    def own_load(matrix):
        source = (w_value, w_gate, w_out)[matrix % 3]
        return pltpu.make_async_copy(
            source.at[matrix // 3],
            weights.at[matrix, pl.ds(aligned(sp * depth, 16), depth), :],
            load_sem.at[matrix],
        )

    for matrix in range(layers * 3):
        own_load(matrix).start()

    def piece(block, m, quarter):
        start = block * depth + ((m % subs) * groups + quarter) * part
        return weights.at[m // subs, pl.ds(aligned(start, 16), part), :]

    def z_copy(way, m, hop, block):
        ref = piece(block, m, grp)
        return pltpu.make_async_remote_copy(
            src_ref=ref,
            dst_ref=ref,
            send_sem=z_send.at[way, m, hop],
            recv_sem=z_recv.at[way, m, hop],
            device_id={"sp": sp + 1 if way == 0 else sp - 1},
            device_id_type=MESH,
        )

    def y_copy(m, block, off, quarter):
        ref = piece(block, m, quarter)
        return pltpu.make_async_remote_copy(
            src_ref=ref,
            dst_ref=ref,
            send_sem=y_send.at[m, block, off - 1],
            recv_sem=y_recv.at[m, block, off - 1],
            device_id={"grp": (grp + off) % groups},
            device_id_type=MESH,
        )

    def send_own(m):
        @pl.when(sp < n - 1)
        def _():
            z_copy(0, m, 0, sp).start()

        @pl.when(sp > 0)
        def _():
            z_copy(1, m, 0, sp).start()

    def weight_step(k):
        m, r = k // hops, k % hops

        @pl.when(sp - (r + 1) >= 0)
        def _():
            block = sp - (r + 1)
            z_copy(0, m, r, block).wait_recv()

            @pl.when(sp < n - 1)
            def _():
                z_copy(0, m, r + 1, block).start()

            for off in range(1, groups):
                y_copy(m, block, off, grp).start()

        @pl.when(sp + (r + 1) < n)
        def _():
            block = sp + (r + 1)
            z_copy(1, m, r, block).wait_recv()

            @pl.when(sp > 0)
            def _():
                z_copy(1, m, r + 1, block).start()

            for off in range(1, groups):
                y_copy(m, block, off, grp).start()

        @pl.when(jnp.logical_and(r == hops - 1, m + 2 < pieces))
        def _():
            send_own(m + 2)

    def weight_steps(low, high):
        lax.fori_loop(low, high, lambda k, c: (weight_step(k), c)[1], 0)

    def weight_share(low, high, i):
        span = high - low
        weight_steps(low + span * i // chunks, low + span * (i + 1) // chunks)

    def matrix_wait(matrix):
        def wait(i, c):
            m, block = matrix * subs + i // n, i % n

            @pl.when(block != sp)
            def _():
                for off in range(1, groups):
                    y_copy(m, block, off, (grp + groups - off) % groups).wait_recv()

            return c

        lax.fori_loop(0, subs * n, wait, 0)

    def chunk_rows(c):
        return pl.ds(aligned(c * rows, rows), rows)

    def x_copy(phase, c, source, slot, target):
        ref = gathered.at[phase, chunk_rows(c), pl.ds(aligned(source * cols, LANES), cols)]
        return pltpu.make_async_remote_copy(
            src_ref=ref,
            dst_ref=ref,
            send_sem=x_send.at[phase, c, slot],
            recv_sem=x_recv.at[phase, c, source],
            device_id={"tp": target},
            device_id_type=MESH,
        )

    def x_own(phase, c):
        for off in range(1, chips):
            x_copy(phase, c, me, off - 1, ((chip + off) % chips) * 2 + core).start()
        x_copy(phase, c, me, chips - 1, partner).start()

    def x_forward(phase, c):
        for off in range(1, chips):
            source = ((chip + off) % chips) * 2 + core
            x_copy(phase, c, source, 0, partner).wait_recv()
            x_copy(phase, c, source, chips - 1 + off, partner).start()

    def x_wait(phase, c):
        for off in range(chips):
            source = ((chip + off) % chips) * 2 + 1 - core
            x_copy(phase, c, source, 0, partner).wait_recv()

    def s_copy(phase, c, source, slot, target):
        ref = stats.at[phase, c, source]
        return pltpu.make_async_remote_copy(
            src_ref=ref,
            dst_ref=ref,
            send_sem=s_send.at[phase, c, slot],
            recv_sem=s_recv.at[phase, c, source],
            device_id={"tp": target},
            device_id_type=MESH,
        )

    def s_share(phase, c, first, second):
        lane = lax.broadcasted_iota(jnp.int32, (rows, LANES), 1)
        both = jnp.where(lane < 4, first, second)
        stats[phase, c, me] = both.T[:8]
        for off in range(1, tp):
            s_copy(phase, c, me, off - 1, (me + off) % tp).start()

    def s_total(phase, c):
        for off in range(1, tp):
            s_copy(phase, c, (me + off) % tp, 0, me).wait_recv()
        total = stats[phase, c, 0]
        for source in range(1, tp):
            total = total + stats[phase, c, source]
        return jnp.concatenate([total] * (LANES // 8), axis=0).T

    def h_copy(layer, way):
        if way == 0:
            source, target, device = count, 0, sp + 1
        else:
            source, target, device = HALO, HALO + count, sp - 1
        return pltpu.make_async_remote_copy(
            src_ref=glu.at[layer, pl.ds(source, HALO), :],
            dst_ref=glu.at[layer, pl.ds(target, HALO), :],
            send_sem=h_send.at[layer, way],
            recv_sem=h_recv.at[layer, way],
            device_id={"sp": device},
            device_id_type=MESH,
        )

    mine = pl.ds(aligned(me * cols, LANES), cols)

    def share_stream(layer, c, wide):
        s_share(2 * layer, c, jnp.sum(wide * wide, axis=1, keepdims=True), 0.0)
        gain = norm_gain[pl.ds(layer, 1), mine]
        gathered[2 * layer, chunk_rows(c), mine] = (wide * gain).astype(bf16)
        x_own(2 * layer, c)

    def loop(function):
        lax.fori_loop(0, chunks, lambda i, c: (function(i), c)[1], 0)

    def inner_first(i):
        return (1 + 2 * i) % chunks

    def ends_first(i):
        return (2 * i) % chunks

    for layer in range(layers):

        @pl.when(sp == 0)
        def _():
            glu[layer, pl.ds(0, HALO), :] = jnp.zeros((HALO, cols), bf16)

        @pl.when(sp == n - 1)
        def _():
            glu[layer, pl.ds(HALO + count, HALO), :] = jnp.zeros((HALO, cols), bf16)

    for matrix in range(layers * 3):
        own_load(matrix).wait()
    pl.semaphore_wait(
        barrier,
        tp - 1 + groups - 1 + (sp > 0).astype(jnp.int32) + (sp < n - 1).astype(jnp.int32),
    )
    send_own(0)
    send_own(1)

    loop(lambda c: share_stream(0, c, tokens[chunk_rows(c), :].astype(f32)))

    def gated(layer, low, high, i):
        c = ends_first(i)
        phase = 2 * layer
        scale = lax.rsqrt(s_total(phase, c)[:, :1] / width + 1e-06)
        block = gathered[phase, chunk_rows(c), :]
        value = jnp.dot(block, weights[3 * layer], preferred_element_type=f32) * scale
        gate = jnp.dot(block, weights[3 * layer + 1], preferred_element_type=f32) * scale
        glu[layer, pl.ds(aligned(HALO + c * rows, HALO), rows), :] = (
            value * jax.nn.sigmoid(gate)
        ).astype(bf16)

        @pl.when(jnp.logical_and(c == 0, sp > 0))
        def _():
            h_copy(layer, 1).start()

        @pl.when(jnp.logical_and(c == chunks - 1, sp < n - 1))
        def _():
            h_copy(layer, 0).start()

        weight_share(low, high, i)

    shift = HALO - half
    groups_of_8 = (kernel + shift + 7) // 8
    window = BLOCK + 8 * groups_of_8

    def convolve(layer, c):
        lane_blocks = cols // LANES

        def block(i, carry):
            base = aligned(c * rows + (i // lane_blocks) * BLOCK, BLOCK)
            lanes = pl.ds(aligned((i % lane_blocks) * LANES, LANES), LANES)
            values = glu[layer, pl.ds(base, window), lanes].astype(f32)
            total = None
            for j in range(8):
                partial = None
                for g in range(groups_of_8):
                    tap = 8 * g + j - shift
                    if tap < 0 or tap >= kernel:
                        continue
                    term = taps[layer, pl.ds(tap, 1), lanes] * values[8 * g : 8 * g + BLOCK + 8]
                    partial = term if partial is None else partial + term
                piece_j = partial[j : j + BLOCK]
                total = piece_j if total is None else total + piece_j
            conv[pl.ds(base, BLOCK), lanes] = total
            return carry

        lax.fori_loop(0, rows // BLOCK * lane_blocks, block, 0)

    def mixed(layer, low, high, i):
        c = inner_first(i)

        @pl.when(jnp.logical_and(c == 0, sp > 0))
        def _():
            h_copy(layer, 0).wait_recv()

        @pl.when(jnp.logical_and(c == chunks - 1, sp < n - 1))
        def _():
            h_copy(layer, 1).wait_recv()

        convolve(layer, c)
        whole = conv[chunk_rows(c), :]
        s_share(
            2 * layer + 1,
            c,
            jnp.sum(whole, axis=1, keepdims=True),
            jnp.sum(whole * whole, axis=1, keepdims=True),
        )
        weight_share(low, high, i)

    def activate(layer, i):
        c = inner_first(i)
        total = s_total(2 * layer + 1, c)
        mean = total[:, :1] / width
        var = total[:, 4:5] / width - mean * mean
        gain = ln_gain[pl.ds(layer, 1), :]
        moved = ln_shift[pl.ds(layer, 1), :]
        shaped = (conv[chunk_rows(c), :] - mean) * lax.rsqrt(var + 1e-05) * gain + moved
        act = shaped * jax.nn.sigmoid(shaped)
        gathered[2 * layer + 1, chunk_rows(c), mine] = act.astype(bf16)
        x_own(2 * layer + 1, c)

    def close(layer, low, high, i):
        c = inner_first(i)
        phase = 2 * layer + 1
        x_forward(phase, c)
        x_wait(phase, c)
        update = jnp.dot(
            gathered[phase, chunk_rows(c), :],
            weights[3 * layer + 2],
            preferred_element_type=f32,
        )
        source = tokens if layer == 0 else out
        stream = (source[chunk_rows(c), :].astype(f32) + update).astype(bf16)
        out[chunk_rows(c), :] = stream
        if layer + 1 < layers:
            share_stream(layer + 1, c, stream.astype(f32))
            weight_share(low, high, i)

    def arrive(layer, low, high, i):
        c = i if layer == 0 else inner_first(i)
        x_forward(2 * layer, c)
        x_wait(2 * layer, c)
        weight_share(low, high, i)

    for layer in range(layers):
        first = 3 * layer * per_matrix
        if layer == 0:
            loop(functools.partial(arrive, layer, first, first + 2 * per_matrix))
        else:
            loop(functools.partial(arrive, layer, first + per_matrix, first + 2 * per_matrix))
        matrix_wait(3 * layer)
        matrix_wait(3 * layer + 1)
        closing = first + 2 * per_matrix
        middle = closing + per_matrix // 2
        loop(functools.partial(gated, layer, closing, middle))
        loop(functools.partial(mixed, layer, middle, closing + per_matrix))
        loop(functools.partial(activate, layer))
        matrix_wait(3 * layer + 2)
        after = closing + per_matrix
        loop(functools.partial(close, layer, after, after + per_matrix))

    def drain_weights(i, carry):
        m, block = i // n, i % n

        @pl.when(block <= sp)
        def _():
            @pl.when(sp < n - 1)
            def _():
                z_copy(0, m, sp - block, block).wait_send()

        @pl.when(block >= sp)
        def _():
            @pl.when(sp > 0)
            def _():
                z_copy(1, m, block - sp, block).wait_send()

        @pl.when(block != sp)
        def _():
            for off in range(1, groups):
                y_copy(m, block, off, grp).wait_send()

        return carry

    lax.fori_loop(0, pieces * n, drain_weights, 0)

    def drain_chunks(i, carry):
        phase, c = i // chunks, i % chunks
        for slot in range(tp - 1):
            x_copy(phase, c, me, slot, partner).wait_send()
            s_copy(phase, c, me, slot, partner).wait_send()
        return carry

    lax.fori_loop(0, 2 * layers * chunks, drain_chunks, 0)
    for layer in range(layers):

        @pl.when(sp < n - 1)
        def _():
            h_copy(layer, 0).wait_send()

        @pl.when(sp > 0)
        def _():
            h_copy(layer, 1).wait_send()


def solution(mesh):
    groups, n, tp = mesh.shape["grp"], mesh.shape["sp"], mesh.shape["tp"]

    def shards(tokens, norm_gain, w_value, w_gate, taps, ln_gain, ln_shift, w_out):
        layers, depth, cols = w_value.shape
        count = tokens.shape[0]
        chunks = 3
        subs = 2 if depth >= 512 else 1
        pieces = layers * 3 * subs
        rows = count // chunks
        vmem = pl.BlockSpec(memory_space=pltpu.VMEM)
        hbm = pl.BlockSpec(memory_space=pl.ANY)
        dma = pltpu.SemaphoreType.DMA
        return pl.pallas_call(
            functools.partial(body, (groups, n, tp, chunks, subs)),
            out_shape=jax.ShapeDtypeStruct((count, cols), jnp.bfloat16),
            in_specs=[vmem, vmem, hbm, hbm, vmem, vmem, vmem, hbm],
            out_specs=vmem,
            scratch_shapes=[
                pltpu.VMEM((layers * 3, depth * n, cols), jnp.bfloat16),
                pltpu.VMEM((2 * layers, count, cols * tp), jnp.bfloat16),
                pltpu.VMEM((layers, count + 2 * HALO, cols), jnp.bfloat16),
                pltpu.VMEM((count, cols), jnp.float32),
                pltpu.VMEM((2 * layers, chunks, tp, 8, rows), jnp.float32),
                dma((layers * 3,)),
                dma((2, pieces, n - 1)),
                dma((2, pieces, n - 1)),
                dma((pieces, n, groups - 1)),
                dma((pieces, n, groups - 1)),
                dma((2 * layers, chunks, tp - 1)),
                dma((2 * layers, chunks, tp)),
                dma((2 * layers, chunks, tp - 1)),
                dma((2 * layers, chunks, tp)),
                dma((layers, 2)),
                dma((layers, 2)),
            ],
            compiler_params=pltpu.CompilerParams(
                collective_id=0, has_side_effects=True, vmem_limit_bytes=60 * 1024 * 1024
            ),
        )(tokens, norm_gain, w_value, w_gate, taps, ln_gain, ln_shift, w_out)

    return jax.shard_map(
        shards,
        mesh=mesh,
        in_specs=(
            P(("grp", "sp"), "tp"),
            P(),
            P(None, "sp", "tp"),
            P(None, "sp", "tp"),
            P(None, None, "tp"),
            P(None, "tp"),
            P(None, "tp"),
            P(None, "sp", "tp"),
        ),
        out_specs=P(("grp", "sp"), "tp"),
        check_vma=False,
    )
```

time: 419 us -> 160 us (0.38)
  waiting for transfers between devices: 335 us -> 0 us
  Pallas kernels: 0 us -> 157 us
  matrix products: 24.7 us -> 0 us
  other arithmetic: 22.5 us -> 0 us
  blocking collectives: 14.1 us -> 0 us
  between operations: 13.8 us -> 0.01 us
  starting transfers between devices: 7.4 us -> 0 us
    all_gather x7 -> x0, waiting for transfers between devices: 326 us -> none  [the longest x1 79.1 us: shards(): lax.all_gather(w_gate, 'sp', axis=1, tiled=True)]
    pallas_call x0 -> x1, Pallas kernels: none -> 157 us  [shards(): pl.pallas_call(functools.partial(body, (groups, n, tp, chunks, subs)), ou...]
    dot_general x6 -> x0, matrix products: 24.7 us -> none  [the longest x2 10.4 us: shards(): jnp.dot(lax.all_gather(act, 'tp', axis=1, tiled=True), out_rows, preferre...]
    reduce_sum x4 -> x0, other arithmetic: 19 us -> none  [the longest x2 13.5 us: shards(): jnp.sum(conv, axis=1)]
    psum x2 -> x0, blocking collectives: 14.1 us -> none  [shards(): lax.psum((jnp.sum(conv, axis=1), jnp.sum(conv * conv, axis=1)), 'tp')]
    ppermute x4 -> x0, starting transfers between devices: 6.98 us -> none  [the longest x2 4.4 us: padded_2(): lax.ppermute(lax.slice_in_dim(block, block.shape[dim] - width, None, axis...]
    ppermute x4 -> x0, waiting for transfers between devices: 6.32 us -> none  [the longest x2 6.31 us: padded_2(): lax.ppermute(lax.slice_in_dim(block, 0, width, axis=dim), axis, backward)]
  transfers between devices with their start and end apart: 11 -> 0, of which waited for: 9 -> 0; matrix products, arithmetic and copies ran while one was open for 5% -> 0% of each run, Pallas kernels for 0% -> 0%
where the time goes in v1:
time: 160 us
  Pallas kernels  157 us (98%)
  local copies, waits for them, and re-layouts  3.65 us (2%)
    pallas_call x1, Pallas kernels, shards(): pl.pallas_call(functools.partial(body, (groups, n, tp, chunks, subs)), ou...  157 us
    unnamed x2, local copies, waits for them, and re-layouts  3.65 us

profile of v1, /device:TPU:1, one launch (start us, length us, event | category | flops | bytes accessed | tf_op | source)
XLA Modules:
  0.0 160.2 jit_solution(15810193143824275846)
XLA Ops:
  0.0 1.6 copy.9.taps
  1.6 156.6 %shard_map.82 = bf16[768,512]{1,0:T(8,128)(2,1)} custom-call(bf16[768,512]{1,0:T(8,128)(2,1)} %tokens.1, f32[2,2048]{1,0:T(2,128)} %norm_gain.1, bf16[2,512,512]{2,1,0:T(8,128)(2,1)} %w_value.1, bf16[2,512,512]{2,1,0:T(8,128)(2,1)} %w_gate.1, f32[2,31,512]{2,1,0:T(8,128)} %copy.9.taps, f32[2,512]{1,0:T(2,128)} %ln_gain.1, f32[2,512]{1,0:T(2,128)} %ln_shift.1, ...), custom_call_target="tpu_custom_call" | custom-call | tf_op jit(solution)/shard_map/pallas_call | solution.py:464
  158.2 2.1 %copy.11 = bf16[768,512]{1,0:T(8,128)(2,1)} copy(bf16[768,512]{1,0:T(8,128)(2,1)} %shard_map.82) | data formatting | bytes 1572864

commit v2 on v1

--- a/solution.py
+++ b/solution.py
@@ -11,6 +11,7 @@
 HALO = 16
 LANES = 128
 BLOCK = 64
+LEAD = 4
 
 
 def body(
@@ -19,11 +20,12 @@
     norm_gain,
     w_value,
     w_gate,
-    taps,
+    taps_in,
     ln_gain,
     ln_shift,
     w_out,
     out,
+    taps,
     weights,
     gathered,
     glu,
@@ -41,13 +43,13 @@
     h_send,
     h_recv,
 ):
-    groups, n, tp, chunks, subs = sizes
+    groups, n, tp, chunks, subs, ahead = sizes
     chips = tp // 2
     grp, sp, me = lax.axis_index("grp"), lax.axis_index("sp"), lax.axis_index("tp")
     chip, core = me // 2, me % 2
     partner = chip * 2 + 1 - core
     layers, depth, cols = w_value.shape
-    kernel = taps.shape[1]
+    kernel = taps_in.shape[1]
     half = (kernel - 1) // 2
     count = tokens.shape[0]
     rows = count // chunks
@@ -56,6 +58,7 @@
     part = depth // (groups * subs)
     hops = n - 1
     per_matrix = subs * hops
+    lead = LEAD
     f32, bf16 = jnp.float32, jnp.bfloat16
 
     def aligned(value, unit):
@@ -87,8 +90,10 @@
             load_sem.at[matrix],
         )
 
+    taps_load = pltpu.make_async_copy(taps_in, taps, load_sem.at[layers * 3])
     for matrix in range(layers * 3):
         own_load(matrix).start()
+    taps_load.start()
 
     def piece(block, m, quarter):
         start = block * depth + ((m % subs) * groups + quarter) * part
@@ -152,9 +157,9 @@
             for off in range(1, groups):
                 y_copy(m, block, off, grp).start()
 
-        @pl.when(jnp.logical_and(r == hops - 1, m + 2 < pieces))
-        def _():
-            send_own(m + 2)
+        @pl.when(jnp.logical_and(r == hops - 1, m + ahead < pieces))
+        def _():
+            send_own(m + ahead)
 
     def weight_steps(low, high):
         lax.fori_loop(low, high, lambda k, c: (weight_step(k), c)[1], 0)
@@ -275,12 +280,13 @@
 
     for matrix in range(layers * 3):
         own_load(matrix).wait()
+    taps_load.wait()
     pl.semaphore_wait(
         barrier,
         tp - 1 + groups - 1 + (sp > 0).astype(jnp.int32) + (sp < n - 1).astype(jnp.int32),
     )
-    send_own(0)
-    send_own(1)
+    for m in range(ahead):
+        send_own(m)
 
     loop(lambda c: share_stream(0, c, tokens[chunk_rows(c), :].astype(f32)))
 
@@ -388,22 +394,26 @@
         x_wait(2 * layer, c)
         weight_share(low, high, i)
 
+    def due(k):
+        return min(k + lead, pieces * hops)
+
     for layer in range(layers):
         first = 3 * layer * per_matrix
-        if layer == 0:
-            loop(functools.partial(arrive, layer, first, first + 2 * per_matrix))
-        else:
-            loop(functools.partial(arrive, layer, first + per_matrix, first + 2 * per_matrix))
+        closing = first + 2 * per_matrix
+        early = due(closing + per_matrix // 6)
+        middle = due(closing + per_matrix // 2)
+        after = due(closing + per_matrix)
+        closing = due(closing)
+        opening = 0 if layer == 0 else due(first + per_matrix)
+        loop(functools.partial(arrive, layer, opening, closing))
         matrix_wait(3 * layer)
         matrix_wait(3 * layer + 1)
-        closing = first + 2 * per_matrix
-        middle = closing + per_matrix // 2
-        loop(functools.partial(gated, layer, closing, middle))
-        loop(functools.partial(mixed, layer, middle, closing + per_matrix))
+        loop(functools.partial(gated, layer, closing, early))
+        loop(functools.partial(mixed, layer, early, middle))
         loop(functools.partial(activate, layer))
+        weight_steps(middle, after)
         matrix_wait(3 * layer + 2)
-        after = closing + per_matrix
-        loop(functools.partial(close, layer, after, after + per_matrix))
+        loop(functools.partial(close, layer, after, due(first + 4 * per_matrix)))
 
     def drain_weights(i, carry):
         m, block = i // n, i % n
@@ -456,23 +466,25 @@
         count = tokens.shape[0]
         chunks = 3
         subs = 2 if depth >= 512 else 1
+        ahead = 2
         pieces = layers * 3 * subs
         rows = count // chunks
         vmem = pl.BlockSpec(memory_space=pltpu.VMEM)
         hbm = pl.BlockSpec(memory_space=pl.ANY)
         dma = pltpu.SemaphoreType.DMA
         return pl.pallas_call(
-            functools.partial(body, (groups, n, tp, chunks, subs)),
+            functools.partial(body, (groups, n, tp, chunks, subs, ahead)),
             out_shape=jax.ShapeDtypeStruct((count, cols), jnp.bfloat16),
-            in_specs=[vmem, vmem, hbm, hbm, vmem, vmem, vmem, hbm],
+            in_specs=[vmem, vmem, hbm, hbm, hbm, vmem, vmem, hbm],
             out_specs=vmem,
             scratch_shapes=[
+                pltpu.VMEM(taps.shape, jnp.float32),
                 pltpu.VMEM((layers * 3, depth * n, cols), jnp.bfloat16),
                 pltpu.VMEM((2 * layers, count, cols * tp), jnp.bfloat16),
                 pltpu.VMEM((layers, count + 2 * HALO, cols), jnp.bfloat16),
                 pltpu.VMEM((count, cols), jnp.float32),
                 pltpu.VMEM((2 * layers, chunks, tp, 8, rows), jnp.float32),
-                dma((layers * 3,)),
+                dma((layers * 3 + 1,)),
                 dma((2, pieces, n - 1)),
                 dma((2, pieces, n - 1)),
                 dma((pieces, n, groups - 1)),

time: 160 us -> 150 us (0.938)
  Pallas kernels: 157 us -> 146 us
    pallas_call x1, Pallas kernels: 157 us -> 146 us  [shards(): pl.pallas_call(functools.partial(body, (groups, n, tp, chunks, subs, ahea...]
where the time goes in v2:
time: 150 us
  Pallas kernels  146 us (97%)
  local copies, waits for them, and re-layouts  3.65 us (2%)
    pallas_call x1, Pallas kernels, shards(): pl.pallas_call(functools.partial(body, (groups, n, tp, chunks, subs, ahea...  146 us
    unnamed x2, local copies, waits for them, and re-layouts  3.65 us

profile of v2, /device:TPU:1, one launch (start us, length us, event | category | flops | bytes accessed | tf_op | source)
XLA Modules:
  0.0 150.1 jit_solution(10590572883804128225)
XLA Ops:
  0.0 1.6 %copy.9.taps_in = f32[2,31,512]{2,1,0:T(8,128)} copy(f32[2,31,512]{2,0,1:T(2,128)} %param.12) | data formatting | bytes 253952 | tf_op args[4]
  1.6 146.4 %shard_map.82 = bf16[768,512]{1,0:T(8,128)(2,1)} custom-call(bf16[768,512]{1,0:T(8,128)(2,1)} %tokens.1, f32[2,2048]{1,0:T(2,128)} %norm_gain.1, bf16[2,512,512]{2,1,0:T(8,128)(2,1)} %w_value.1, bf16[2,512,512]{2,1,0:T(8,128)(2,1)} %w_gate.1, f32[2,31,512]{2,1,0:T(8,128)} %copy.9.taps_in, f32[2,512]{1,0:T(2,128)} %ln_gain.1, f32[2,512]{1,0:T(2,128)} %ln_shift.1, ...), custom_call_target="tpu_custom_call" | custom-call | tf_op jit(solution)/shard_map/pallas_call | solution.py:475
  148.0 2.1 %copy.11 = bf16[768,512]{1,0:T(8,128)(2,1)} copy(bf16[768,512]{1,0:T(8,128)(2,1)} %shard_map.82) | data formatting | bytes 1572864
